TPU v7x, 32 devices: a whole 2x2x4 slice. The times are simulated.
32 devices in a mesh: ep: 8 (over z, y), tp: 4 (over x, core).
Axes of the slice: x: 2, y: 2, z: 4, core: 2. Of those that a mesh axis runs over, the one named last changes fastest.
Arguments:
- tokens: bfloat16 [128, 2048], P('ep', 'tp'), may hold values from -40 to 40
- kv_cache: bfloat16 [128, 1024, 512], P('ep', None, 'tp'), may hold values from -1000 to 1000
- cum_gate: float32 [128, 16, 1024], P('ep', 'tp'), may hold values from -400 to 0, as said below
- lengths: int32 [128], P('ep'), may hold values from 256 to 1024
- w_query: bfloat16 [2048, 1024], P(None, 'tp'), may hold values from -0.125 to 0.125
- w_key: bfloat16 [2048, 256], P(None, 'tp'), may hold values from -0.125 to 0.125
- w_value: bfloat16 [2048, 256], P(None, 'tp'), may hold values from -0.125 to 0.125
- w_forget: bfloat16 [2048, 16], P(None, 'tp'), may hold values from -0.5 to 0.5
- forget_bias: float32 [16], P('tp'), may hold values from -2.5 to 1.5
- w_out: bfloat16 [1024, 2048], P('tp'), may hold values from -0.1875 to 0.1875
- attn_gain: bfloat16 [2048], replicated, may hold values from 0.099609375 to 1.8984375
- ffn_gain: bfloat16 [2048], replicated, may hold values from 0.099609375 to 1.8984375
- mix_gate: bfloat16 [2048], replicated, may hold values from -0.125 to 0.125
- expert_gate: bfloat16 [8, 2048, 1024], P('ep', None, 'tp'), may hold values from -0.125 to 0.125
- expert_up: bfloat16 [8, 2048, 1024], P('ep', None, 'tp'), may hold values from -0.125 to 0.125
- expert_down: bfloat16 [8, 1024, 2048], P('ep', 'tp'), may hold values from -0.1875 to 0.1875
- chosen: int32 [128, 2], P('ep'), may hold values from 0 to 7, as said below
- route_weight: float32 [128, 2], P('ep'), may hold values from 0.5 to 1.5
- dense_gate: bfloat16 [2048, 1024], P(None, 'tp'), may hold values from -0.125 to 0.125
- dense_up: bfloat16 [2048, 1024], P(None, 'tp'), may hold values from -0.125 to 0.125
- dense_down: bfloat16 [1024, 2048], P('tp'), may hold values from -0.1875 to 0.1875
Outputs:
- mixed: bfloat16 [128, 2048], P('ep', 'tp')
Inputs may be any that keep to these rules, and one draw needn't show every extreme that they name: `cum_gate`: along positions each row never rises: entry p is the sum of the log forget gates of positions 0 to p of that sequence and head. `chosen`: each row names two different experts of one group of 8 consecutive expert numbers. The rows of one device name any one expert at most 8 times, and some expert exactly 8 times.
All inputs are finite; a program needn't handle non-finite values.
Results may differ from a plain program's by a relative error of at most 0.014.
Values may be sent and summed in bfloat16 or wider, within the bound.
A program may use at most 64 MiB of HBM per device.

v0:
```python
import jax
import jax.numpy as jnp
from jax import lax
from jax.sharding import PartitionSpec as P

HD = 64
TOP = 2
epsilon = 1e-06


def norm_rows(values, scales):
    widened = values.astype(jnp.float32)
    square = jnp.mean(widened * widened, axis=-1, keepdims=True)
    return (widened * lax.rsqrt(square + epsilon) * scales.astype(jnp.float32)).astype(jnp.bfloat16)


def attend(h_one, kv_cache, cum_gate, lengths, w_query, w_key, w_value, w_forget, forget_bias):
    tok_count = h_one.shape[0]
    cache_len = kv_cache.shape[1]
    kv_local = w_key.shape[1] // HD
    q_local = w_query.shape[1] // HD
    group_size = q_local // kv_local
    score_scale = HD ** (-0.5)
    queries = jnp.dot(h_one, w_query, preferred_element_type=jnp.float32).astype(jnp.bfloat16)
    queries = queries.reshape(tok_count, kv_local, group_size, HD)
    key_new = jnp.dot(h_one, w_key, preferred_element_type=jnp.float32).astype(jnp.bfloat16)
    key_new = key_new.reshape(tok_count, kv_local, HD)
    value_new = jnp.dot(h_one, w_value, preferred_element_type=jnp.float32).astype(jnp.bfloat16)
    value_new = value_new.reshape(tok_count, kv_local, HD)
    forget_now = jax.nn.log_sigmoid(
        jnp.dot(h_one, w_forget, preferred_element_type=jnp.float32) + forget_bias
    )
    forget_now = forget_now.reshape(tok_count, kv_local, group_size)
    stacked = kv_cache.reshape(tok_count, cache_len, kv_local, 2, HD)
    past_keys = stacked[:, :, :, 0, :]
    past_values = stacked[:, :, :, 1, :]
    scores = (
        jnp.einsum("sjgd,scjd->sjgc", queries, past_keys, preferred_element_type=jnp.float32)
        * score_scale
    )
    cumulative = cum_gate.reshape(tok_count, kv_local, group_size, cache_len)
    position_rows = jnp.arange(cache_len, dtype=jnp.int32)
    at_last = (position_rows[None, :] == (lengths - 1)[:, None]).astype(jnp.float32)
    latest = jnp.sum(cumulative * at_last[:, None, None, :], axis=-1, keepdims=True)
    scores = scores + latest - cumulative + forget_now[:, :, :, None]
    inside = position_rows[None, :] < lengths[:, None]
    scores = jnp.where(inside[:, None, None, :], scores, -jnp.inf)
    own_score = (
        jnp.einsum("sjgd,sjd->sjg", queries, key_new, preferred_element_type=jnp.float32)
        * score_scale
    )
    highest = jnp.maximum(jnp.max(scores, axis=-1), own_score)
    weights = jnp.exp(scores - highest[:, :, :, None])
    own_weight = jnp.exp(own_score - highest)
    denominator = jnp.sum(weights, axis=-1) + own_weight
    weights = (weights / denominator[:, :, :, None]).astype(jnp.bfloat16)
    own_weight = (own_weight / denominator).astype(jnp.bfloat16)
    blended = jnp.einsum(
        "sjgc,scjd->sjgd", weights, past_values, preferred_element_type=jnp.float32
    )
    blended = (
        blended
        + own_weight.astype(jnp.float32)[:, :, :, None]
        * value_new.astype(jnp.float32)[:, :, None, :]
    )
    return blended.astype(jnp.bfloat16).reshape(tok_count, q_local * HD)


def local(
    tokens,
    kv_cache,
    cum_gate,
    lengths,
    w_query,
    w_key,
    w_value,
    w_forget,
    forget_bias,
    w_out,
    attn_gain,
    ffn_gain,
    mix_gate,
    expert_gate,
    expert_up,
    expert_down,
    chosen,
    route_weight,
    dense_gate,
    dense_up,
    dense_down,
):
    tok_count = tokens.shape[0]
    slice_width = tokens.shape[1]
    ep_count = lax.axis_size("ep")
    gathered = lax.all_gather(tokens, "tp", axis=1, tiled=True)
    model_width = gathered.shape[1]
    h_one = norm_rows(gathered, attn_gain)
    head_out = attend(
        h_one, kv_cache, cum_gate, lengths, w_query, w_key, w_value, w_forget, forget_bias
    )
    partial_value = jnp.dot(head_out, w_out, preferred_element_type=jnp.float32)
    tp_offset = lax.axis_index("tp") * slice_width
    attention = lax.psum(partial_value.astype(jnp.bfloat16), "tp").astype(jnp.float32)
    residual_full = (gathered.astype(jnp.float32) + attention).astype(jnp.bfloat16)
    h_two = norm_rows(residual_full, ffn_gain)
    residual = lax.dynamic_slice_in_dim(residual_full, tp_offset, slice_width, 1)
    capacity = max(2, (4 * tok_count + ep_count - 1) // ep_count)
    routes = chosen.reshape(-1)
    expert_ids = jnp.arange(ep_count, dtype=jnp.int32)
    one_hot = (routes[:, None] == expert_ids[None, :]).astype(jnp.int32)
    rank_of = jnp.sum((jnp.cumsum(one_hot, axis=0) - one_hot) * one_hot, axis=1)
    slot_of = routes * capacity + rank_of
    slot_ids = jnp.arange(ep_count * capacity, dtype=jnp.int32)
    chooser = (slot_ids[:, None] == slot_of[None, :]).astype(jnp.bfloat16)
    per_token = jnp.sum(chooser.reshape(ep_count * capacity, tok_count, TOP), axis=2)
    outgoing = jnp.dot(per_token, h_two, preferred_element_type=jnp.float32).astype(jnp.bfloat16)
    outgoing = outgoing.reshape(ep_count, capacity, model_width)
    received = lax.all_to_all(outgoing, "ep", split_axis=0, concat_axis=0, tiled=True)
    flat_rows = received.reshape(-1, model_width)
    gate_pre = jnp.dot(flat_rows, expert_gate[0], preferred_element_type=jnp.float32)
    up_pre = jnp.dot(flat_rows, expert_up[0], preferred_element_type=jnp.float32)
    hidden = (jax.nn.silu(gate_pre) * up_pre).astype(jnp.bfloat16)
    part_out = jnp.dot(hidden, expert_down[0], preferred_element_type=jnp.float32)
    summed = lax.psum_scatter(part_out.astype(jnp.bfloat16), "tp", scatter_dimension=1, tiled=True)
    shares = summed.reshape(received.shape[0], received.shape[1], -1)
    returned = lax.all_to_all(shares, "ep", split_axis=0, concat_axis=0, tiled=True)
    returned = returned.reshape(ep_count * capacity, slice_width)
    picked = jnp.dot(chooser.T, returned, preferred_element_type=jnp.float32)
    routed_sum = jnp.sum(
        picked.reshape(tok_count, TOP, slice_width) * route_weight[:, :, None], axis=1
    )
    dense_pre = jnp.dot(h_two, dense_gate, preferred_element_type=jnp.float32)
    dense_lift = jnp.dot(h_two, dense_up, preferred_element_type=jnp.float32)
    dense_act = (jax.nn.silu(dense_pre) * dense_lift).astype(jnp.bfloat16)
    dense_part = jnp.dot(dense_act, dense_down, preferred_element_type=jnp.float32)
    dense_out = lax.psum_scatter(
        dense_part.astype(jnp.bfloat16), "tp", scatter_dimension=1, tiled=True
    ).astype(jnp.float32)
    blend_gate = jax.nn.sigmoid(jnp.dot(h_two, mix_gate, preferred_element_type=jnp.float32))
    return (residual.astype(jnp.float32) + routed_sum + blend_gate[:, None] * dense_out).astype(
        jnp.bfloat16
    )


def solution(mesh):
    in_specs = (
        P("ep", "tp"),
        P("ep", None, "tp"),
        P("ep", "tp", None),
        P("ep"),
        P(None, "tp"),
        P(None, "tp"),
        P(None, "tp"),
        P(None, "tp"),
        P("tp"),
        P("tp", None),
        P(),
        P(),
        P(),
        P("ep", None, "tp"),
        P("ep", None, "tp"),
        P("ep", "tp", None),
        P("ep", None),
        P("ep", None),
        P(None, "tp"),
        P(None, "tp"),
        P("tp", None),
    )
    out_specs = P("ep", "tp")
    return jax.shard_map(local, mesh=mesh, in_specs=in_specs, out_specs=out_specs, check_vma=False)
```

profile of v0, /device:TPU:0, one launch (start us, length us, event | category | flops | bytes accessed | tf_op | source)
XLA Modules:
  0.0 130.5 jit_solution(5122951195548866926)
XLA Ops:
  6.5 6.6 %all_gather.3 = bf16[16,2048]{1,0:T(8,128)(2,1)S(1)} all-gather(bf16[16,512]{1,0:T(8,128)(2,1)} %param.21), channel_id=1, replica_groups=mesh['ep'=8,'tp'=4] {'tp'}, dimensions={1}, use_global_device_ids=true | all-gather | bytes 81920 | tf_op jit(solution)/shard_map/all_gather | solution.py:95
  13.1 0.1 fusion.34
  13.3 0.7 convert_element_type.98
  13.9 1.5 %convolution_convert_fusion.4 = bf16[16,256]{1,0:T(8,128)(2,1)S(1)} fusion(bf16[2048,256]{1,0:T(8,128)(2,1)} %param.25, bf16[16,2048]{1,0:T(8,128)(2,1)S(1)} %all_gather.3, f32[2048]{0:T(1024)S(1)} %convert_element_type.98, f32[16]{0:T(128)S(1)} %add_rsqrt_fusion.1), kind=kOutput, calls=%fused_computation.23 | convolution fusion | flops 16912384 | bytes 1130560 | tf_op jit(solution)/shard_map/dot_general | solution.py:24
  15.6 6.5 %copy.43 = bf16[16,1024,128]{1,2,0:T(8,128)(2,1)} copy(bf16[16,1024,128]{2,1,0:T(8,128)(2,1)} %param.22) | data formatting | bytes 8388608 | tf_op args[1]
  22.1 0.2 fusion.63
  22.5 0.2 fusion.15
  22.7 2.2 %fusion.8 = f32[16,4,1024]{2,1,0:T(4,128)S(1)} fusion(bf16[16,4,64]{2,1,0:T(4,128)(2,1)S(1)} %reshape.204, bf16[16,1024,1,2,64]{1,4,3,0,2:T(8,128)(2,1)} %bitcast.68), kind=kOutput, calls=%fused_computation.14 | convolution fusion | flops 8454144 | bytes 2367488 | tf_op jit(solution)/shard_map/sjgd,scjd->sjgc/dot_general | solution.py:38
  24.9 0.1 fusion.59
  25.1 0.3 fusion.77
  25.4 0.2 fusion.30
  25.7 0.2 fusion.14
  25.9 0.7 fusion.12
  26.7 2.2 %convolution_convert_fusion.3 = bf16[16,2048]{1,0:T(8,128)(2,1)} fusion(bf16[16,256]{1,0:T(8,128)(2,1)S(1)} %reshape.208, bf16[256,2048]{1,0:T(8,128)(2,1)} %param.30), kind=kOutput, calls=%fused_computation.5 | convolution fusion | flops 16809984 | bytes 1122304 | tf_op jit(solution)/shard_map/dot_general | solution.py:101
  29.3 0.2 select_reduce_fusion
  29.8 32.6 %all-reduce.2.cloned.1.call-done = bf16[16,2048]{1,0:T(8,128)(2,1)} async-done(((bf16[16,2048]{1,0:T(8,128)(2,1)}), bf16[16,2048]{1,0:T(8,128)(2,1)}) %all-reduce.2.cloned.1.call-update) | async-done | bytes 65552 | tf_op jit(solution)/shard_map/psum | solution.py:103
  62.4 1.0 fusion.31
  63.4 1.0 fusion.1
  64.3 5.5 %all-to-all-start = ((bf16[8,8,2048]{2,1,0:T(8,128)(2,1)}), bf16[8,8,2048]{2,1,0:T(8,128)(2,1)S(1)}, u32[]{:S(2)}, u32[]{:S(2)}) async-start(bf16[8,8,2048]{2,1,0:T(8,128)(2,1)} %fusion.1), calls=%async_computation | async-start | bytes 524288 | tf_op jit(solution)/shard_map/all_to_all | solution.py:118
  69.9 0.6 reshape.217
  70.6 7.5 %all-to-all-done = bf16[8,8,2048]{2,1,0:T(8,128)(2,1)S(1)} async-done(((bf16[8,8,2048]{2,1,0:T(8,128)(2,1)}), bf16[8,8,2048]{2,1,0:T(8,128)(2,1)S(1)}, u32[]{:S(2)}, u32[]{:S(2)}) %all-to-all-start) | async-done | bytes 262176 | tf_op jit(solution)/shard_map/all_to_all | solution.py:118
  78.1 1.5 %fusion.24 = f32[64,256]{1,0:T(8,128)S(1)} fusion(bf16[1,2048,256]{2,1,0:T(8,128)(2,1)} %param.34, bf16[8,8,2048]{2,1,0:T(8,128)(2,1)S(1)} %all-to-all-done), kind=kOutput, calls=%fused_computation.37 | convolution fusion | flops 67108864 | bytes 1376256 | tf_op jit(solution)/shard_map/dot_general | solution.py:120
  79.6 2.7 %convolution_convert_fusion = bf16[64,2048]{1,0:T(8,128)(2,1)} fusion(bf16[1,256,2048]{2,1,0:T(8,128)(2,1)S(1)} %copy-done, bf16[1,2048,256]{2,1,0:T(8,128)(2,1)} %param.35, bf16[8,8,2048]{2,1,0:T(8,128)(2,1)S(1)} %all-to-all-done, f32[64,256]{1,0:T(8,128)S(1)} %fusion.24), kind=kOutput, calls=%fused_computation.1 | convolution fusion | flops 134447104 | bytes 2686976 | tf_op jit(solution)/shard_map/dot_general | solution.py:123
  82.4 1.5 %fusion.72 = f32[16,256]{1,0:T(8,128)S(1)} fusion(bf16[2048,256]{1,0:T(8,128)(2,1)} %param.39, bf16[16,2048]{1,0:T(8,128)(2,1)S(1)} %get-tuple-element.6, f32[2048]{0:T(1024)S(1)} %convert_element_type.116, f32[16]{0:T(128)} %copy-done.4), kind=kOutput, calls=%fused_computation.102 | convolution fusion | flops 16908288 | bytes 1138752 | tf_op jit(solution)/shard_map/dot_general | solution.py:132
  83.9 2.0 %convolution_convert_fusion.2 = bf16[16,2048]{1,0:T(8,128)(2,1)} fusion(bf16[256,2048]{1,0:T(8,128)(2,1)S(1)} %copy-done.2, bf16[2048,256]{1,0:T(8,128)(2,1)S(1)} %copy-done.3, f32[16,256]{1,0:T(8,128)S(1)} %fusion.72, bf16[16,2048]{1,0:T(8,128)(2,1)S(1)} %get-tuple-element.6, f32[2048]{0:T(1024)S(1)} %convert_element_type.116, f32[16]{0:T(128)} %copy-done.4), kind=kOutput, calls=%fused_computation.4 | convolution fusion | flops 33742848 | bytes 2252864 | tf_op jit(solution)/shard_map/dot_general | solution.py:135
  86.0 14.6 %reduce-scatter.3.cloned.1.call-done = bf16[64,512]{1,0:T(8,128)(2,1)} async-done(((bf16[64,2048]{1,0:T(8,128)(2,1)}), bf16[64,512]{1,0:T(8,128)(2,1)}) %reduce-scatter.3.cloned.1.call-update) | async-done | bytes 65552 | tf_op jit(solution)/shard_map/reduce_scatter | solution.py:124
  100.5 5.5 %all-to-all-start.1 = ((bf16[8,8,512]{2,1,0:T(8,128)(2,1)}), bf16[8,8,512]{2,1,0:T(8,128)(2,1)S(1)}, u32[]{:S(2)}, u32[]{:S(2)}) async-start(bf16[8,8,512]{2,1,0:T(8,128)(2,1)} %bitcast.70), calls=%async_computation.2 | async-start | bytes 131072 | tf_op jit(solution)/shard_map/all_to_all | solution.py:126
  106.0 0.9 fusion.20
  106.9 6.0 %all-to-all-done.1 = bf16[8,8,512]{2,1,0:T(8,128)(2,1)S(1)} async-done(((bf16[8,8,512]{2,1,0:T(8,128)(2,1)}), bf16[8,8,512]{2,1,0:T(8,128)(2,1)S(1)}, u32[]{:S(2)}, u32[]{:S(2)}) %all-to-all-start.1) | async-done | bytes 65568 | tf_op jit(solution)/shard_map/all_to_all | solution.py:126
  112.9 0.8 fusion.10
  113.8 8.8 %reduce-scatter.5.cloned.1.call-done = bf16[16,512]{1,0:T(8,128)(2,1)} async-done(((bf16[16,2048]{1,0:T(8,128)(2,1)}), bf16[16,512]{1,0:T(8,128)(2,1)}) %reduce-scatter.5.cloned.1.call-update) | async-done | bytes 16400 | tf_op jit(solution)/shard_map/reduce_scatter | solution.py:136
  122.5 1.4 %add_convert_fusion = bf16[16,512]{1,0:T(8,128)(2,1)} fusion(bf16[16,512]{1,0:T(8,128)(2,1)} %reduce-scatter.5.cloned.1.call-done, f32[16,512]{1,0:T(8,128)S(1)} %fusion.10, f32[16]{0:T(128)S(1)} %fusion.20, bf16[16,2048]{1,0:T(8,128)(2,1)S(1)} %get-tuple-element.6, s32[]{:T(128)S(6)} %select_n.15), kind=kLoop, calls=%fused_computation.70 | loop fusion | flops 49152 | bytes 81988 | tf_op jit(solution)/shard_map/convert_element_type | solution.py:140
  (55 shorter events, 1.3 us)
Async XLA Ops:
  6.5 73.1 %copy-start = (bf16[1,256,2048]{2,1,0:T(8,128)(2,1)S(1)}, bf16[1,256,2048]{2,1,0:T(8,128)(2,1)}, u32[]{:S(2)}) copy-start(bf16[1,256,2048]{2,1,0:T(8,128)(2,1)} %param.36) | copy-start | bytes 3145732
  6.5 55.8 %all-reduce.2.cloned.1.call-start = ((), (), s32[]{:S(2)}) async-start(), calls=%async_computation.4 | async-start | bytes 131072 | tf_op jit(solution)/shard_map/psum | solution.py:103
  15.5 6.5 %copy-start.12 = (bf16[2048,4]{0,1:T(4,128)(2,1)S(1)}, bf16[2048,4]{0,1:T(4,128)(2,1)}, u32[]{:S(2)}) copy-start(bf16[2048,4]{0,1:T(4,128)(2,1)} %param.28) | copy-start | bytes 49156
  15.6 6.5 %copy-start.13 = (f32[4]{0:T(128)S(1)}, f32[4]{0:T(128)}, u32[]{:S(2)}) copy-start(f32[4]{0:T(128)} %param.29) | copy-start | bytes 52
  15.6 6.8 %copy-start.8 = (s32[16]{0:T(128)S(1)}, s32[16]{0:T(128)}, u32[]{:S(2)}) copy-start(s32[16]{0:T(128)} %param.24) | copy-start | bytes 196
  15.6 6.9 %copy-start.9 = (bf16[2048,64]{0,1:T(8,128)(2,1)S(1)}, bf16[2048,64]{0,1:T(8,128)(2,1)}, u32[]{:S(2)}) copy-start(bf16[2048,64]{0,1:T(8,128)(2,1)} %param.26) | copy-start | bytes 786436
  15.6 9.5 %copy-start.10 = (f32[16,4,1024]{2,1,0:T(4,128)S(1)}, f32[16,4,1024]{2,1,0:T(4,128)}, u32[]{:S(2)}) copy-start(f32[16,4,1024]{2,1,0:T(4,128)} %param.23) | copy-start | bytes 786436
  22.1 3.6 %copy-start.11 = (bf16[2048,64]{0,1:T(8,128)(2,1)S(1)}, bf16[2048,64]{0,1:T(8,128)(2,1)}, u32[]{:S(2)}) copy-start(bf16[2048,64]{0,1:T(8,128)(2,1)} %param.27) | copy-start | bytes 786436
  22.4 3.5 %copy-start.1 = (bf16[16,1024,128]{1,2,0:T(8,128)(2,1)S(1)}, bf16[16,1024,128]{1,2,0:T(8,128)(2,1)}, u32[]{:S(2)}) copy-start(bf16[16,1024,128]{1,2,0:T(8,128)(2,1)} %copy.43) | copy-start | bytes 12582916
  24.9 4.1 %copy-start.7 = (s32[16,2]{0,1:T(2,128)S(1)}, s32[16,2]{0,1:T(2,128)}, u32[]{:S(2)}) copy-start(s32[16,2]{0,1:T(2,128)} %param.37) | copy-start | bytes 388
  24.9 4.8 %copy-start.5 = (bf16[2048]{0:T(1024)(128)(2,1)S(1)}, bf16[2048]{0:T(1024)(128)(2,1)}, u32[]{:S(2)}) copy-start(bf16[2048]{0:T(1024)(128)(2,1)} %param.32) | copy-start | bytes 12292
  25.1 44.8 %copy-start.6 = (bf16[2048]{0:T(1024)(128)(2,1)S(1)}, bf16[2048]{0:T(1024)(128)(2,1)}, u32[]{:S(2)}) copy-start(bf16[2048]{0:T(1024)(128)(2,1)} %param.33) | copy-start | bytes 12292
  26.6 57.3 %copy-start.2 = (bf16[256,2048]{1,0:T(8,128)(2,1)S(1)}, bf16[256,2048]{1,0:T(8,128)(2,1)}, u32[]{:S(2)}) copy-start(bf16[256,2048]{1,0:T(8,128)(2,1)} %param.41) | copy-start | bytes 3145732
  26.6 57.3 %copy-start.3 = (bf16[2048,256]{1,0:T(8,128)(2,1)S(1)}, bf16[2048,256]{1,0:T(8,128)(2,1)}, u32[]{:S(2)}) copy-start(bf16[2048,256]{1,0:T(8,128)(2,1)} %param.40) | copy-start | bytes 3145732
  63.4 1.0 copy-start.4
  64.3 13.7 %all-to-all-start = ((bf16[8,8,2048]{2,1,0:T(8,128)(2,1)}), bf16[8,8,2048]{2,1,0:T(8,128)(2,1)S(1)}, u32[]{:S(2)}, u32[]{:S(2)}) async-start(bf16[8,8,2048]{2,1,0:T(8,128)(2,1)} %fusion.1), calls=%async_computation | async-start | bytes 524288 | tf_op jit(solution)/shard_map/all_to_all | solution.py:118
  69.9 30.7 %reduce-scatter.3.cloned.1.call-start = ((), (), s32[]{:S(2)}) async-start(), calls=%async_computation.5 | async-start | bytes 327680 | tf_op jit(solution)/shard_map/reduce_scatter | solution.py:124
  82.4 40.2 %reduce-scatter.5.cloned.1.call-start = ((), (), s32[]{:S(2)}) async-start(), calls=%async_computation.6 | async-start | bytes 81920 | tf_op jit(solution)/shard_map/reduce_scatter | solution.py:136
  100.5 12.4 %all-to-all-start.1 = ((bf16[8,8,512]{2,1,0:T(8,128)(2,1)}), bf16[8,8,512]{2,1,0:T(8,128)(2,1)S(1)}, u32[]{:S(2)}, u32[]{:S(2)}) async-start(bf16[8,8,512]{2,1,0:T(8,128)(2,1)} %bitcast.70), calls=%async_computation.2 | async-start | bytes 131072 | tf_op jit(solution)/shard_map/all_to_all | solution.py:126
Sparse Core Ops, SparseCore 0:
  29.1 33.2 all-reduce.1
  82.5 18.0 reduce-scatter.2
  103.0 19.5 reduce-scatter.4
where the time goes:
time: 131 us; the launch traced here: 130 us
  waiting for transfers between devices  69.4 us (53%)
  matrix products  17.9 us (14%)
  between operations  13.3 us (10%)
  starting transfers between devices  11.1 us (8%)
  local copies, waits for them, and re-layouts  7.77 us (6%)
  blocking collectives  6.57 us (5%)
  other arithmetic  4.38 us (3%)
    psum x1, waiting for transfers between devices, local(): lax.psum(partial_value.astype(jnp.bfloat16), 'tp').astype(jnp.float32)  32.6 us
    reduce_scatter x1, waiting for transfers between devices, local(): lax.psum_scatter(part_out.astype(jnp.bfloat16), 'tp', scatter_dimension=1...  14.6 us
    reduce_scatter x1, waiting for transfers between devices, local(): lax.psum_scatter(dense_part.astype(jnp.bfloat16), 'tp', scatter_dimension...  8.77 us
    all_to_all x1, waiting for transfers between devices, local(): lax.all_to_all(outgoing, 'ep', split_axis=0, concat_axis=0, tiled=True)  7.45 us
    unnamed x31, local copies, waits for them, and re-layouts  7.22 us
    all_gather x1, blocking collectives, local(): gathered = lax.all_gather(tokens, 'tp', axis=1, tiled=True)  6.57 us
    all_to_all x1, waiting for transfers between devices, local(): lax.all_to_all(shares, 'ep', split_axis=0, concat_axis=0, tiled=True)  6 us
    all_to_all x1, starting transfers between devices, local(): lax.all_to_all(outgoing, 'ep', split_axis=0, concat_axis=0, tiled=True)  5.52 us
  transfers between devices with their start and end apart: 5, of which 5 were waited for; matrix products, arithmetic and copies ran while one was open for 5% of the time, Pallas kernels for 0%

commit v1 on v0

--- a/solution.py
+++ b/solution.py
@@ -100,7 +100,9 @@
     )
     partial_value = jnp.dot(head_out, w_out, preferred_element_type=jnp.float32)
     tp_offset = lax.axis_index("tp") * slice_width
-    attention = lax.psum(partial_value.astype(jnp.bfloat16), "tp").astype(jnp.float32)
+    attention = jnp.sum(lax.all_gather(partial_value.astype(jnp.bfloat16), "tp"), axis=0).astype(
+        jnp.float32
+    )
     residual_full = (gathered.astype(jnp.float32) + attention).astype(jnp.bfloat16)
     h_two = norm_rows(residual_full, ffn_gain)
     residual = lax.dynamic_slice_in_dim(residual_full, tp_offset, slice_width, 1)

time: 131 us -> 108 us (0.82)
  waiting for transfers between devices: 69.4 us -> 30.2 us
  blocking collectives: 6.57 us -> 27.9 us
  starting transfers between devices: 11.1 us -> 5.56 us
  matrix products: 17.9 us -> 15.3 us
  other arithmetic: 4.38 us -> 6.38 us
    psum x1 -> x0, waiting for transfers between devices: 32.6 us -> none  [local(): lax.psum(partial_value.astype(jnp.bfloat16), 'tp').astype(jnp.float32)]
    all_to_all x0 -> x1, blocking collectives: none -> 15.2 us  [local(): lax.all_to_all(outgoing, 'ep', split_axis=0, concat_axis=0, tiled=True)]
    all_to_all x1 -> x0, waiting for transfers between devices: 7.45 us -> none  [local(): lax.all_to_all(outgoing, 'ep', split_axis=0, concat_axis=0, tiled=True)]
    all_gather x0 -> x1, blocking collectives: none -> 6.21 us  [local(): lax.all_gather(partial_value.astype(jnp.bfloat16), 'tp')]
    all_to_all x1 -> x0, starting transfers between devices: 5.52 us -> none  [local(): lax.all_to_all(outgoing, 'ep', split_axis=0, concat_axis=0, tiled=True)]
    add x2, other arithmetic: 0.01 us -> 1.36 us  [local(): slot_of = routes * capacity + rank_of]
    unnamed x31 -> x27, local copies, waits for them, and re-layouts: 7.22 us -> 7.98 us
  transfers between devices with their start and end apart: 5 -> 3, of which waited for: 5 -> 3; matrix products, arithmetic and copies ran while one was open for 5% -> 5% of each run, Pallas kernels for 0% -> 0%
where the time goes in v1:
time: 108 us; the launch traced here: 107 us
  waiting for transfers between devices  30.2 us (28%)
  blocking collectives  27.9 us (26%)
  matrix products  15.3 us (14%)
  between operations  13.6 us (13%)
  local copies, waits for them, and re-layouts  8.52 us (8%)
  other arithmetic  6.38 us (6%)
  starting transfers between devices  5.56 us (5%)
    all_to_all x1, blocking collectives, local(): lax.all_to_all(outgoing, 'ep', split_axis=0, concat_axis=0, tiled=True)  15.2 us
    reduce_scatter x1, waiting for transfers between devices, local(): lax.psum_scatter(part_out.astype(jnp.bfloat16), 'tp', scatter_dimension=1...  14.6 us
    reduce_scatter x1, waiting for transfers between devices, local(): lax.psum_scatter(dense_part.astype(jnp.bfloat16), 'tp', scatter_dimension...  8.75 us
    unnamed x27, local copies, waits for them, and re-layouts  7.98 us
    all_to_all x1, waiting for transfers between devices, local(): lax.all_to_all(shares, 'ep', split_axis=0, concat_axis=0, tiled=True)  6.81 us
    all_gather x1, blocking collectives, local(): gathered = lax.all_gather(tokens, 'tp', axis=1, tiled=True)  6.57 us
    all_gather x1, blocking collectives, local(): lax.all_gather(partial_value.astype(jnp.bfloat16), 'tp')  6.21 us
    all_to_all x1, starting transfers between devices, local(): lax.all_to_all(shares, 'ep', split_axis=0, concat_axis=0, tiled=True)  5.52 us
  transfers between devices with their start and end apart: 3, of which 3 were waited for; matrix products, arithmetic and copies ran while one was open for 5% of the time, Pallas kernels for 0%

profile of v1, /device:TPU:0, one launch (start us, length us, event | category | flops | bytes accessed | tf_op | source)
XLA Modules:
  0.0 107.5 jit_solution(16837346550059615981)
XLA Ops:
  6.5 6.6 %all_gather.9 = bf16[16,2048]{1,0:T(8,128)(2,1)S(1)} all-gather(bf16[16,512]{1,0:T(8,128)(2,1)} %param.21), channel_id=1, replica_groups=mesh['ep'=8,'tp'=4] {'tp'}, dimensions={1}, use_global_device_ids=true | all-gather | bytes 81920 | tf_op jit(solution)/shard_map/all_gather | solution.py:95
  13.3 0.7 convert_element_type.100
  13.9 1.5 %convolution_convert_fusion.4 = bf16[16,256]{1,0:T(8,128)(2,1)S(1)} fusion(bf16[2048,256]{1,0:T(8,128)(2,1)} %param.25, bf16[16,2048]{1,0:T(8,128)(2,1)S(1)} %all_gather.9, f32[2048]{0:T(1024)S(1)} %convert_element_type.100, f32[16]{0:T(128)S(1)} %add_rsqrt_fusion.1), kind=kOutput, calls=%fused_computation.23 | convolution fusion | flops 16912384 | bytes 1130560 | tf_op jit(solution)/shard_map/dot_general | solution.py:24
  15.6 6.5 %copy.43 = bf16[16,1024,128]{1,2,0:T(8,128)(2,1)} copy(bf16[16,1024,128]{2,1,0:T(8,128)(2,1)} %param.22) | data formatting | bytes 8388608 | tf_op args[1]
  22.1 0.2 fusion.63
  22.5 0.2 fusion.15
  22.7 2.2 %fusion.8 = f32[16,4,1024]{2,1,0:T(4,128)S(1)} fusion(bf16[16,4,64]{2,1,0:T(4,128)(2,1)S(1)} %reshape.204, bf16[16,1024,1,2,64]{1,4,3,0,2:T(8,128)(2,1)} %bitcast.69), kind=kOutput, calls=%fused_computation.14 | convolution fusion | flops 8454144 | bytes 2367488 | tf_op jit(solution)/shard_map/sjgd,scjd->sjgc/dot_general | solution.py:38
  25.0 0.3 fusion.77
  25.4 0.2 fusion.30
  25.7 0.2 fusion.14
  25.9 0.7 fusion.12
  26.7 1.6 %convolution_convert_fusion.3 = bf16[16,2048]{1,0:T(8,128)(2,1)S(1)} fusion(bf16[16,256]{1,0:T(8,128)(2,1)S(1)} %reshape.208, bf16[256,2048]{1,0:T(8,128)(2,1)} %param.30), kind=kOutput, calls=%fused_computation.5 | convolution fusion | flops 16809984 | bytes 1122304 | tf_op jit(solution)/shard_map/dot_general | solution.py:101
  28.3 6.2 %all-gather = bf16[64,2048]{1,0:T(8,128)(2,1)S(1)} all-gather(bf16[16,2048]{1,0:T(8,128)(2,1)S(1)} %convolution_convert_fusion.3), channel_id=2, replica_groups=mesh['ep'=8,'tp'=4] {'tp'}, dimensions={0}, use_global_device_ids=true | all-gather | bytes 327680 | tf_op jit(solution)/shard_map/all_gather | solution.py:103
  34.6 0.7 reduce_sum.83
  35.2 1.0 fusion.31
  36.2 0.8 copy.47
  37.6 0.7 multiply_add_fusion
  38.3 0.3 fusion.1
  38.6 15.2 %all_to_all.10 = bf16[8,8,2048]{2,1,0:T(8,128)(2,1)S(1)} all-to-all(bf16[8,8,2048]{2,1,0:T(8,128)(2,1)S(1)} %fusion.1), channel_id=1, replica_groups=mesh['ep'=8,'tp'=4] {'ep'}, dimensions={0} | all-to-all | bytes 524288 | tf_op jit(solution)/shard_map/all_to_all | solution.py:120
  53.8 1.5 %fusion.24 = f32[64,256]{1,0:T(8,128)S(1)} fusion(bf16[1,2048,256]{2,1,0:T(8,128)(2,1)} %param.34, bf16[8,8,2048]{2,1,0:T(8,128)(2,1)S(1)} %all_to_all.10), kind=kOutput, calls=%fused_computation.37 | convolution fusion | flops 67108864 | bytes 1376256 | tf_op jit(solution)/shard_map/dot_general | solution.py:122
  55.3 2.7 %convolution_convert_fusion = bf16[64,2048]{1,0:T(8,128)(2,1)} fusion(bf16[1,256,2048]{2,1,0:T(8,128)(2,1)S(1)} %copy-done, bf16[1,2048,256]{2,1,0:T(8,128)(2,1)} %param.35, bf16[8,8,2048]{2,1,0:T(8,128)(2,1)S(1)} %all_to_all.10, f32[64,256]{1,0:T(8,128)S(1)} %fusion.24), kind=kOutput, calls=%fused_computation.1 | convolution fusion | flops 134447104 | bytes 2686976 | tf_op jit(solution)/shard_map/dot_general | solution.py:125
  58.1 1.5 %fusion.72 = f32[16,256]{1,0:T(8,128)S(1)} fusion(bf16[2048,256]{1,0:T(8,128)(2,1)} %param.39, bf16[16,2048]{1,0:T(8,128)(2,1)S(1)} %get-tuple-element.6, f32[2048]{0:T(1024)S(1)} %convert_element_type.118, f32[16]{0:T(128)S(1)} %add_rsqrt_fusion), kind=kOutput, calls=%fused_computation.102 | convolution fusion | flops 16908288 | bytes 1138752 | tf_op jit(solution)/shard_map/dot_general | solution.py:134
  59.6 1.4 %convolution_convert_fusion.2 = bf16[16,2048]{1,0:T(8,128)(2,1)} fusion(bf16[256,2048]{1,0:T(8,128)(2,1)S(1)} %copy-done.2, bf16[2048,256]{1,0:T(8,128)(2,1)S(1)} %copy-done.3, f32[16,256]{1,0:T(8,128)S(1)} %fusion.72, bf16[16,2048]{1,0:T(8,128)(2,1)S(1)} %get-tuple-element.6, f32[2048]{0:T(1024)S(1)} %convert_element_type.118, f32[16]{0:T(128)S(1)} %add_rsqrt_fusion), kind=kOutput, calls=%fused_computation.4 | convolution fusion | flops 33742848 | bytes 2252864 | tf_op jit(solution)/shard_map/dot_general | solution.py:137
  61.1 0.7 multiply_add_fusion.1
  61.7 0.7 reshape.218
  62.4 0.2 fusion.20
  62.6 14.6 %reduce-scatter.3.cloned.1.call-done = bf16[64,512]{1,0:T(8,128)(2,1)} async-done(((bf16[64,2048]{1,0:T(8,128)(2,1)}), bf16[64,512]{1,0:T(8,128)(2,1)}) %reduce-scatter.3.cloned.1.call-update) | async-done | bytes 65552 | tf_op jit(solution)/shard_map/reduce_scatter | solution.py:126
  77.2 5.5 %all-to-all-start.1 = ((bf16[8,8,512]{2,1,0:T(8,128)(2,1)}), bf16[8,8,512]{2,1,0:T(8,128)(2,1)S(1)}, u32[]{:S(2)}, u32[]{:S(2)}) async-start(bf16[8,8,512]{2,1,0:T(8,128)(2,1)} %bitcast.72), calls=%async_computation.2 | async-start | bytes 131072 | tf_op jit(solution)/shard_map/all_to_all | solution.py:128
  82.8 6.8 %all-to-all-done.1 = bf16[8,8,512]{2,1,0:T(8,128)(2,1)S(1)} async-done(((bf16[8,8,512]{2,1,0:T(8,128)(2,1)}), bf16[8,8,512]{2,1,0:T(8,128)(2,1)S(1)}, u32[]{:S(2)}, u32[]{:S(2)}) %all-to-all-start.1) | async-done | bytes 65568 | tf_op jit(solution)/shard_map/all_to_all | solution.py:128
  89.7 0.8 fusion.10
  90.5 8.8 %reduce-scatter.5.cloned.1.call-done = bf16[16,512]{1,0:T(8,128)(2,1)} async-done(((bf16[16,2048]{1,0:T(8,128)(2,1)}), bf16[16,512]{1,0:T(8,128)(2,1)}) %reduce-scatter.5.cloned.1.call-update) | async-done | bytes 16400 | tf_op jit(solution)/shard_map/reduce_scatter | solution.py:138
  99.2 1.4 %add_convert_fusion = bf16[16,512]{1,0:T(8,128)(2,1)} fusion(bf16[16,512]{1,0:T(8,128)(2,1)} %reduce-scatter.5.cloned.1.call-done, f32[16,512]{1,0:T(8,128)S(1)} %fusion.10, f32[16]{0:T(128)S(1)} %fusion.20, bf16[16,2048]{1,0:T(8,128)(2,1)S(1)} %get-tuple-element.6, s32[]{:T(128)S(6)} %select_n.15), kind=kLoop, calls=%fused_computation.70 | loop fusion | flops 49152 | bytes 81988 | tf_op jit(solution)/shard_map/convert_element_type | solution.py:142
  (49 shorter events, 1.5 us)
Async XLA Ops:
  6.5 48.8 %copy-start = (bf16[1,256,2048]{2,1,0:T(8,128)(2,1)S(1)}, bf16[1,256,2048]{2,1,0:T(8,128)(2,1)}, u32[]{:S(2)}) copy-start(bf16[1,256,2048]{2,1,0:T(8,128)(2,1)} %param.36) | copy-start | bytes 3145732
  6.5 70.7 %reduce-scatter.3.cloned.1.call-start = ((), (), s32[]{:S(2)}) async-start(), calls=%async_computation.4 | async-start | bytes 327680 | tf_op jit(solution)/shard_map/reduce_scatter | solution.py:126
  15.5 6.5 %copy-start.10 = (bf16[2048,4]{0,1:T(4,128)(2,1)S(1)}, bf16[2048,4]{0,1:T(4,128)(2,1)}, u32[]{:S(2)}) copy-start(bf16[2048,4]{0,1:T(4,128)(2,1)} %param.28) | copy-start | bytes 49156
  15.6 6.5 %copy-start.11 = (f32[4]{0:T(128)S(1)}, f32[4]{0:T(128)}, u32[]{:S(2)}) copy-start(f32[4]{0:T(128)} %param.29) | copy-start | bytes 52
  15.6 6.8 %copy-start.6 = (s32[16]{0:T(128)S(1)}, s32[16]{0:T(128)}, u32[]{:S(2)}) copy-start(s32[16]{0:T(128)} %param.24) | copy-start | bytes 196
  15.6 6.9 %copy-start.7 = (bf16[2048,64]{0,1:T(8,128)(2,1)S(1)}, bf16[2048,64]{0,1:T(8,128)(2,1)}, u32[]{:S(2)}) copy-start(bf16[2048,64]{0,1:T(8,128)(2,1)} %param.26) | copy-start | bytes 786436
  15.6 9.5 %copy-start.8 = (f32[16,4,1024]{2,1,0:T(4,128)S(1)}, f32[16,4,1024]{2,1,0:T(4,128)}, u32[]{:S(2)}) copy-start(f32[16,4,1024]{2,1,0:T(4,128)} %param.23) | copy-start | bytes 786436
  22.1 3.6 %copy-start.9 = (bf16[2048,64]{0,1:T(8,128)(2,1)S(1)}, bf16[2048,64]{0,1:T(8,128)(2,1)}, u32[]{:S(2)}) copy-start(bf16[2048,64]{0,1:T(8,128)(2,1)} %param.27) | copy-start | bytes 786436
  22.4 3.5 %copy-start.1 = (bf16[16,1024,128]{1,2,0:T(8,128)(2,1)S(1)}, bf16[16,1024,128]{1,2,0:T(8,128)(2,1)}, u32[]{:S(2)}) copy-start(bf16[16,1024,128]{1,2,0:T(8,128)(2,1)} %copy.43) | copy-start | bytes 12582916
  24.9 11.3 %copy-start.4 = (bf16[2048]{0:T(1024)(128)(2,1)S(1)}, bf16[2048]{0:T(1024)(128)(2,1)}, u32[]{:S(2)}) copy-start(bf16[2048]{0:T(1024)(128)(2,1)} %param.32) | copy-start | bytes 12292
  26.7 32.9 %copy-start.2 = (bf16[256,2048]{1,0:T(8,128)(2,1)S(1)}, bf16[256,2048]{1,0:T(8,128)(2,1)}, u32[]{:S(2)}) copy-start(bf16[256,2048]{1,0:T(8,128)(2,1)} %param.41) | copy-start | bytes 3145732
  26.7 32.9 %copy-start.3 = (bf16[2048,256]{1,0:T(8,128)(2,1)S(1)}, bf16[2048,256]{1,0:T(8,128)(2,1)}, u32[]{:S(2)}) copy-start(bf16[2048,256]{1,0:T(8,128)(2,1)} %param.40) | copy-start | bytes 3145732
  37.4 1.0 copy-start.5
  58.0 41.2 %reduce-scatter.5.cloned.1.call-start = ((), (), s32[]{:S(2)}) async-start(), calls=%async_computation.5 | async-start | bytes 81920 | tf_op jit(solution)/shard_map/reduce_scatter | solution.py:138
  77.2 12.4 %all-to-all-start.1 = ((bf16[8,8,512]{2,1,0:T(8,128)(2,1)}), bf16[8,8,512]{2,1,0:T(8,128)(2,1)S(1)}, u32[]{:S(2)}, u32[]{:S(2)}) async-start(bf16[8,8,512]{2,1,0:T(8,128)(2,1)} %bitcast.72), calls=%async_computation.2 | async-start | bytes 131072 | tf_op jit(solution)/shard_map/all_to_all | solution.py:128
Sparse Core Ops, SparseCore 0:
  58.2 19.0 reduce-scatter.2
  79.6 19.5 reduce-scatter.4
